TPU v7x, 32 devices: a whole 2x2x4 slice. The times are simulated.
32 devices in a mesh: kv: 8 (over z, y), tp: 4 (over x, core).
Axes of the slice: x: 2, y: 2, z: 4, core: 2. Of those that a mesh axis runs over, the one named last changes fastest.
Arguments:
- tokens: bfloat16 [8192, 1024], P('kv', 'tp'), may hold values from -6 to 6
- query_weight: bfloat16 [1024, 2048], P(None, 'tp'), may hold values from -0.1875 to 0.1875
- latent_weight: bfloat16 [1024, 128], replicated, may hold values from -0.1875 to 0.1875
- query_gain: float32 [128], replicated, may hold values from 0.5 to 1.5
- key_gain: float32 [128], replicated, may hold values from 0.5 to 1.5
- value_up: bfloat16 [16, 128, 64], P('tp'), may hold values from -0.5 to 0.5
- out_weight: bfloat16 [1024, 1024], P('tp'), may hold values from -0.25 to 0.25
- out_gain: float32 [1024], replicated, may hold values from 0.5 to 1.5
- chosen: int32 [64, 32], P('kv'), may hold values from -1 to 63, as said below
Outputs:
- mixed_out: bfloat16 [8192, 1024], P('kv', 'tp')
Inputs may be any that keep to these rules, and one draw needn't show every extreme that they name: Row b lists the key blocks chosen for query block b: entry 0 is b itself, then distinct blocks before b, then -1 in every unused place. Block j is held by index j // 8 of kv. All query blocks of one index of kv together choose at most 2 distinct blocks held by any one other index, and some pair of indices reaches that bound; blocks held by the same index are chosen freely.
All inputs are finite; a program needn't handle non-finite values.
Results may differ from a plain program's by a relative error of at most 0.02.
Values may be sent and summed in bfloat16 or wider, within the bound.
A program may use at most 64 MiB of HBM per device.

v0:
```python
import jax
import jax.numpy as jnp
from jax import lax
from jax.sharding import PartitionSpec as P

BLOCK = 128
PER_OWNER = 2


epsilon = 1e-06
masked_score = -1e30


def taken_in(shard, axis, dim, absorb, carry):
    whole = jax.tree.map(lambda part: lax.all_gather(part, axis, axis=dim, tiled=True), shard)
    return absorb(carry, whole, jnp.int32(0))


def own_rows(product, rows, axis):
    everything = product(jnp.int32(0), lax.axis_size(axis) * rows)
    own = lax.psum_scatter(everything.astype(jnp.bfloat16), axis, scatter_dimension=0, tiled=True)
    return own.astype(jnp.float32)


def rms_scale(values, gain_row):
    widened = values.astype(jnp.float32)
    mean_sq = jnp.mean(widened * widened, axis=-1, keepdims=True)
    return (widened * lax.rsqrt(mean_sq + epsilon) * gain_row).astype(jnp.bfloat16)


def on_device(
    tokens,
    query_weight,
    latent_weight,
    query_gain,
    key_gain,
    value_up,
    out_weight,
    out_gain,
    chosen,
):
    tok_rows = tokens.shape[0]
    head_cols = query_weight.shape[1]
    lat_width = latent_weight.shape[1]
    local_heads = head_cols // lat_width
    block_size = BLOCK
    blocks_dev = tok_rows // block_size
    owners = lax.axis_size("kv")
    my_owner = lax.axis_index("kv")

    def project(totals, shard_piece, offset):
        query_rows = lax.dynamic_slice_in_dim(query_weight, offset, shard_piece.shape[1], 0)
        latent_rows = lax.dynamic_slice_in_dim(latent_weight, offset, shard_piece.shape[1], 0)
        return (
            totals[0] + jnp.dot(shard_piece, query_rows, preferred_element_type=jnp.float32),
            totals[1] + jnp.dot(shard_piece, latent_rows, preferred_element_type=jnp.float32),
        )

    query_zero = jnp.zeros((tok_rows, head_cols), jnp.float32)
    latent_zero = jnp.zeros((tok_rows, lat_width), jnp.float32)
    query_acc, latent_acc = taken_in(tokens, "tp", 1, project, (query_zero, latent_zero))
    queries = rms_scale(
        query_acc.astype(jnp.bfloat16).reshape(tok_rows, local_heads, lat_width), query_gain
    )
    latent = latent_acc.astype(jnp.bfloat16)
    latent_blocks = latent.reshape(blocks_dev, block_size, lat_width)
    clamped = jnp.maximum(chosen, 0)
    owner_of = clamped // blocks_dev
    index_in = clamped % blocks_dev
    flat_owner = owner_of.reshape(-1)
    flat_index = index_in.reshape(-1)
    remote = (chosen.reshape(-1) >= 0) & (flat_owner != my_owner)
    owner_ids = jnp.arange(owners, dtype=jnp.int32)
    local_ids = jnp.arange(blocks_dev, dtype=jnp.int32)
    matches = (
        remote[:, None, None]
        & (flat_owner[:, None, None] == owner_ids[None, :, None])
        & (flat_index[:, None, None] == local_ids[None, None, :])
    )
    needed = jnp.any(matches, axis=0)
    ranking = jnp.cumsum(needed.astype(jnp.int32), axis=1) - 1
    slot_ids = jnp.arange(PER_OWNER, dtype=jnp.int32)
    placed = needed[:, None, :] & (ranking[:, None, :] == slot_ids[None, :, None])
    wanted = jnp.where(
        jnp.any(placed, axis=2), jnp.sum(jnp.where(placed, local_ids[None, None, :], 0), axis=2), -1
    )
    requested = lax.all_to_all(wanted, "kv", split_axis=0, concat_axis=0, tiled=True)
    served = latent_blocks[jnp.maximum(requested, 0)]
    served = jnp.where((requested >= 0)[:, :, None, None], served, jnp.zeros_like(served))
    arrived = lax.all_to_all(served, "kv", split_axis=0, concat_axis=0, tiled=True)
    block_pool = jnp.concatenate(
        [latent_blocks, arrived.reshape(owners * PER_OWNER, block_size, lat_width)], axis=0
    )
    slot_of = jnp.sum(jnp.where(wanted[owner_of] == index_in[:, :, None], slot_ids, 0), axis=2)
    where_from = jnp.where(
        owner_of == my_owner, index_in, blocks_dev + owner_of * PER_OWNER + slot_of
    )
    selected = block_pool[where_from]
    score_scale = lat_width ** (-0.5)
    offsets = jnp.arange(block_size, dtype=jnp.int32)
    query_blocks = queries.reshape(blocks_dev, block_size, local_heads, lat_width)
    block_starts = my_owner * tok_rows + jnp.arange(blocks_dev, dtype=jnp.int32) * block_size

    def attend(packed):
        query_block, picked_values, chosen_row, start_pos = packed
        picked_keys = rms_scale(picked_values, key_gain)
        scores = (
            jnp.einsum(
                "qhl,ckl->qhck", query_block, picked_keys, preferred_element_type=jnp.float32
            )
            * score_scale
        )
        key_pos = jnp.maximum(chosen_row, 0)[:, None] * block_size + offsets[None, :]
        query_pos = start_pos + offsets
        allowed = (chosen_row[:, None] >= 0)[None] & (key_pos[None] <= query_pos[:, None, None])
        allowed = allowed[:, None]
        scores = jnp.where(allowed, scores, masked_score)
        row_max = jnp.max(scores, axis=(2, 3), keepdims=True)
        exp_scores = jnp.where(allowed, jnp.exp(scores - row_max), 0.0)
        weights = (exp_scores / jnp.sum(exp_scores, axis=(2, 3), keepdims=True)).astype(
            jnp.bfloat16
        )
        attended = jnp.einsum(
            "qhck,ckl->qhl", weights, picked_values, preferred_element_type=jnp.float32
        )
        return attended.astype(jnp.bfloat16)

    attended = lax.map(attend, (query_blocks, selected, chosen, block_starts))
    attended = attended.reshape(tok_rows, local_heads, lat_width)
    heads_out = jnp.einsum("thl,hlv->thv", attended, value_up, preferred_element_type=jnp.float32)
    heads_out = heads_out.astype(jnp.bfloat16).reshape(tok_rows, local_heads * value_up.shape[2])
    model_width = out_weight.shape[1]
    tp_count = lax.axis_size("tp")
    feature_rows = model_width // tp_count
    gain_part = lax.dynamic_slice_in_dim(
        out_gain, lax.axis_index("tp") * feature_rows, feature_rows, 0
    )

    def columns(offset, count):
        weight_cols = lax.dynamic_slice_in_dim(out_weight, offset, count, 1)
        return lax.dot_general(
            weight_cols, heads_out, (((0,), (1,)), ((), ())), preferred_element_type=jnp.float32
        )

    summed = own_rows(columns, feature_rows, "tp").T
    squares = lax.psum(jnp.sum(summed * summed, axis=1), "tp")
    mixed_out = (summed * lax.rsqrt(squares / model_width + epsilon)[:, None] * gain_part).astype(
        jnp.bfloat16
    )
    return mixed_out


def solution(mesh):
    in_specs = (
        P("kv", "tp"),
        P(None, "tp"),
        P(),
        P(),
        P(),
        P("tp", None, None),
        P("tp", None),
        P(),
        P("kv", None),
    )
    out_specs = P("kv", "tp")
    return jax.shard_map(
        on_device, mesh=mesh, in_specs=in_specs, out_specs=out_specs, check_vma=False
    )
```

profile of v0, /device:TPU:29, one launch (start us, length us, event | category | flops | bytes accessed | tf_op | source)
XLA Modules:
  0.0 232.9 jit_solution(9330237730256950675)
XLA Ops:
  6.5 0.7 all-gather.2.cloned.1.call-update
  7.3 0.7 compare_select_fusion.1
  10.4 5.4 %all-to-all-start = ((s32[8,1,2]{2,1,0:T(1,128)}), s32[8,1,2]{2,1,0:T(1,128)S(1)}, u32[]{:S(2)}, u32[]{:S(2)}) async-start(s32[8,1,2]{2,1,0:T(1,128)} %bitcast.27), calls=%async_computation | async-start | bytes 8192 | tf_op jit(solution)/shard_map/all_to_all | solution.py:87
  15.9 1.4 gather_fusion.1
  17.6 0.7 compare_select_fusion
  18.8 14.2 %all-gather.2.cloned.1.call-done = bf16[1024,1024]{1,0:T(8,128)(2,1)} async-done(((bf16[1024,256]{1,0:T(8,128)(2,1)}), bf16[1024,1024]{1,0:T(8,128)(2,1)}) %all-gather.2.cloned.1.call-update) | async-done | bytes 2097168 | tf_op jit(solution)/shard_map/all_gather | solution.py:15
  33.0 2.3 convolution_convert_fusion.2
  35.9 0.9 broadcast_select_fusion
  36.8 5.4 %all-to-all-start.1 = ((bf16[8,2,128,128]{3,2,1,0:T(8,128)(2,1)}), bf16[8,2,128,128]{3,2,1,0:T(8,128)(2,1)}, u32[]{:S(2)}, u32[]{:S(2)}) async-start(bf16[8,2,128,128]{3,2,1,0:T(8,128)(2,1)} %broadcast_select_fusion), calls=%async_computation.1 | async-start | bytes 1048576 | tf_op jit(solution)/shard_map/all_to_all | solution.py:90
  42.3 2.9 %bitcast_reduce_fusion = (f32[1024,4]{0,1:T(4,128)S(1)}, bf16[1024,512]{0,1:T(8,128)(2,1)S(1)}) fusion(bf16[1024,1024]{1,0:T(8,128)(2,1)} %all-gather.2.cloned.1.call-done, bf16[1024,512]{1,0:T(8,128)(2,1)S(1)} %copy-done), kind=kOutput, calls=%fused_computation.39 | convolution fusion | flops 1075834880 | bytes 4210688 | tf_op jit(solution)/shard_map/dot_general | solution.py:55
  45.4 1.8 copy.47
  47.3 1.9 copy.32
  49.2 1.6 multiply_convert_fusion.1
  50.8 4.7 %all-to-all-done.1 = bf16[8,2,128,128]{3,2,1,0:T(8,128)(2,1)} async-done(((bf16[8,2,128,128]{3,2,1,0:T(8,128)(2,1)}), bf16[8,2,128,128]{3,2,1,0:T(8,128)(2,1)}, u32[]{:S(2)}, u32[]{:S(2)}) %all-to-all-start.1) | async-done | bytes 524320 | tf_op jit(solution)/shard_map/all_to_all | solution.py:90
  55.5 1.1 pad_maximum_fusion
  56.6 8.3 %gather_fusion.2 = bf16[256,128,128]{2,1,0:T(8,128)(2,1)} fusion(bf16[24,128,128]{2,1,0:T(8,128)(2,1)S(1)} %pad_maximum_fusion, s32[1024]{0:T(1024)S(1)} %pad_clamp_fusion), kind=kCustom, calls=%fused_computation.2 | custom fusion | bytes 16778240 | tf_op jit(solution)/shard_map/gather | solution.py:98
  65.0 118.2 %while.12 = (s32[]{:T(128)}, bf16[8,128,4,128]{3,1,0,2:T(8,128)(2,1)S(1)}, s32[8,32]{1,0:T(8,128)}, s32[8]{0:T(128)S(1)}, bf16[8,128,4,128]{3,1,2,0:T(8,128)(2,1...) while((s32[]{:T(128)}, ...), condition=%wide.region_10.11_spmd.clone.clone, body=%wide.region_6.10_spmd.clone.clone.sunk | while | flops 1107893504 | bytes 30783664 | solution.py:128
  65.0 0.8 multiply_bitcast_fusion.2
  67.7 0.8 compare_and_fusion.3
  68.5 1.8 multiply_reduce_fusion.2
  70.4 2.8 %fusion.45 = (f32[128,4]{0,1:T(4,128)S(1)}, f32[128,4,32,128]{0,3,2,1:T(8,128)S(1)}) fusion(pred[128,32,128]{0,2,1:T(8,128)(4,1)S(1)} %compare_and_fusion.3, f32[128]{0:T(128)S(1)} %get-tuple-element.179, f32[32,128]{1,0:T(8,128)S(1)} %add_rsqrt_fusion.3, bf16[8,32,128,128]{3,2,1,0:T(8,128)(2,1)} %get-tuple-element.178, s32[]{:T(128)} %get-tuple-element.165, ...), kind=kOutput, calls=%fused_computation.7.clone.1 | convolution fusion | flops 545259008 | bytes 10112512 | tf_op jit(solution)/shard_map/while/body/eval_jaxpr/qhl,ckl->qhck/dot_general | solution.py:108
  73.2 2.1 fusion.46
  75.3 4.5 %fusion.47 = bf16[8,128,4,128]{3,1,0,2:T(8,128)(2,1)S(1)} fusion(bf16[8,128,4,128]{3,1,0,2:T(8,128)(2,1)S(1)} %get-tuple-element.166, s32[]{:T(128)} %get-tuple-element.165, f32[128,4,32,128]{0,3,2,1:T(8,128)S(1)} %get-tuple-element.155, f32[128,4]{0,1:T(4,128)S(1)} %fusion.46, f32[128,4]{0,1:T(4,128)S(1)} %get-tuple-element.156, ...), kind=kOutput, calls=%fused_computation.16.clone.1 | convolution fusion | flops 549519360 | bytes 10097664 | tf_op jit(solution)/shard_map/while/body/eval_jaxpr/qhck,ckl->qhl/dot_general | solution.py:123
  82.5 0.8 compare_and_fusion.3
  83.3 1.8 multiply_reduce_fusion.2
  85.1 2.8 %fusion.45 = (f32[128,4]{0,1:T(4,128)S(1)}, f32[128,4,32,128]{0,3,2,1:T(8,128)S(1)}) fusion(pred[128,32,128]{0,2,1:T(8,128)(4,1)S(1)} %compare_and_fusion.3, f32[128]{0:T(128)S(1)} %get-tuple-element.179, f32[32,128]{1,0:T(8,128)S(1)} %add_rsqrt_fusion.3, bf16[8,32,128,128]{3,2,1,0:T(8,128)(2,1)} %get-tuple-element.178, s32[]{:T(128)} %get-tuple-element.165, ...), kind=kOutput, calls=%fused_computation.7.clone.1 | convolution fusion | flops 545259008 | bytes 10112512 | tf_op jit(solution)/shard_map/while/body/eval_jaxpr/qhl,ckl->qhck/dot_general | solution.py:108
  87.9 2.1 fusion.46
  90.0 4.5 %fusion.47 = bf16[8,128,4,128]{3,1,0,2:T(8,128)(2,1)S(1)} fusion(bf16[8,128,4,128]{3,1,0,2:T(8,128)(2,1)S(1)} %get-tuple-element.166, s32[]{:T(128)} %get-tuple-element.165, f32[128,4,32,128]{0,3,2,1:T(8,128)S(1)} %get-tuple-element.155, f32[128,4]{0,1:T(4,128)S(1)} %fusion.46, f32[128,4]{0,1:T(4,128)S(1)} %get-tuple-element.156, ...), kind=kOutput, calls=%fused_computation.16.clone.1 | convolution fusion | flops 549519360 | bytes 10097664 | tf_op jit(solution)/shard_map/while/body/eval_jaxpr/qhck,ckl->qhl/dot_general | solution.py:123
  97.3 0.8 compare_and_fusion.3
  98.0 1.8 multiply_reduce_fusion.2
  99.9 2.8 %fusion.45 = (f32[128,4]{0,1:T(4,128)S(1)}, f32[128,4,32,128]{0,3,2,1:T(8,128)S(1)}) fusion(pred[128,32,128]{0,2,1:T(8,128)(4,1)S(1)} %compare_and_fusion.3, f32[128]{0:T(128)S(1)} %get-tuple-element.179, f32[32,128]{1,0:T(8,128)S(1)} %add_rsqrt_fusion.3, bf16[8,32,128,128]{3,2,1,0:T(8,128)(2,1)} %get-tuple-element.178, s32[]{:T(128)} %get-tuple-element.165, ...), kind=kOutput, calls=%fused_computation.7.clone.1 | convolution fusion | flops 545259008 | bytes 10112512 | tf_op jit(solution)/shard_map/while/body/eval_jaxpr/qhl,ckl->qhck/dot_general | solution.py:108
  102.7 2.1 fusion.46
  104.8 4.5 %fusion.47 = bf16[8,128,4,128]{3,1,0,2:T(8,128)(2,1)S(1)} fusion(bf16[8,128,4,128]{3,1,0,2:T(8,128)(2,1)S(1)} %get-tuple-element.166, s32[]{:T(128)} %get-tuple-element.165, f32[128,4,32,128]{0,3,2,1:T(8,128)S(1)} %get-tuple-element.155, f32[128,4]{0,1:T(4,128)S(1)} %fusion.46, f32[128,4]{0,1:T(4,128)S(1)} %get-tuple-element.156, ...), kind=kOutput, calls=%fused_computation.16.clone.1 | convolution fusion | flops 549519360 | bytes 10097664 | tf_op jit(solution)/shard_map/while/body/eval_jaxpr/qhck,ckl->qhl/dot_general | solution.py:123
  112.0 0.8 compare_and_fusion.3
  112.8 1.8 multiply_reduce_fusion.2
  114.7 2.8 %fusion.45 = (f32[128,4]{0,1:T(4,128)S(1)}, f32[128,4,32,128]{0,3,2,1:T(8,128)S(1)}) fusion(pred[128,32,128]{0,2,1:T(8,128)(4,1)S(1)} %compare_and_fusion.3, f32[128]{0:T(128)S(1)} %get-tuple-element.179, f32[32,128]{1,0:T(8,128)S(1)} %add_rsqrt_fusion.3, bf16[8,32,128,128]{3,2,1,0:T(8,128)(2,1)} %get-tuple-element.178, s32[]{:T(128)} %get-tuple-element.165, ...), kind=kOutput, calls=%fused_computation.7.clone.1 | convolution fusion | flops 545259008 | bytes 10112512 | tf_op jit(solution)/shard_map/while/body/eval_jaxpr/qhl,ckl->qhck/dot_general | solution.py:108
  117.5 2.1 fusion.46
  119.6 4.5 %fusion.47 = bf16[8,128,4,128]{3,1,0,2:T(8,128)(2,1)S(1)} fusion(bf16[8,128,4,128]{3,1,0,2:T(8,128)(2,1)S(1)} %get-tuple-element.166, s32[]{:T(128)} %get-tuple-element.165, f32[128,4,32,128]{0,3,2,1:T(8,128)S(1)} %get-tuple-element.155, f32[128,4]{0,1:T(4,128)S(1)} %fusion.46, f32[128,4]{0,1:T(4,128)S(1)} %get-tuple-element.156, ...), kind=kOutput, calls=%fused_computation.16.clone.1 | convolution fusion | flops 549519360 | bytes 10097664 | tf_op jit(solution)/shard_map/while/body/eval_jaxpr/qhck,ckl->qhl/dot_general | solution.py:123
  126.8 0.8 compare_and_fusion.3
  127.6 1.8 multiply_reduce_fusion.2
  129.4 2.8 %fusion.45 = (f32[128,4]{0,1:T(4,128)S(1)}, f32[128,4,32,128]{0,3,2,1:T(8,128)S(1)}) fusion(pred[128,32,128]{0,2,1:T(8,128)(4,1)S(1)} %compare_and_fusion.3, f32[128]{0:T(128)S(1)} %get-tuple-element.179, f32[32,128]{1,0:T(8,128)S(1)} %add_rsqrt_fusion.3, bf16[8,32,128,128]{3,2,1,0:T(8,128)(2,1)} %get-tuple-element.178, s32[]{:T(128)} %get-tuple-element.165, ...), kind=kOutput, calls=%fused_computation.7.clone.1 | convolution fusion | flops 545259008 | bytes 10112512 | tf_op jit(solution)/shard_map/while/body/eval_jaxpr/qhl,ckl->qhck/dot_general | solution.py:108
  132.2 2.1 fusion.46
  134.3 4.5 %fusion.47 = bf16[8,128,4,128]{3,1,0,2:T(8,128)(2,1)S(1)} fusion(bf16[8,128,4,128]{3,1,0,2:T(8,128)(2,1)S(1)} %get-tuple-element.166, s32[]{:T(128)} %get-tuple-element.165, f32[128,4,32,128]{0,3,2,1:T(8,128)S(1)} %get-tuple-element.155, f32[128,4]{0,1:T(4,128)S(1)} %fusion.46, f32[128,4]{0,1:T(4,128)S(1)} %get-tuple-element.156, ...), kind=kOutput, calls=%fused_computation.16.clone.1 | convolution fusion | flops 549519360 | bytes 10097664 | tf_op jit(solution)/shard_map/while/body/eval_jaxpr/qhck,ckl->qhl/dot_general | solution.py:123
  141.5 0.8 compare_and_fusion.3
  142.3 1.8 multiply_reduce_fusion.2
  144.2 2.8 %fusion.45 = (f32[128,4]{0,1:T(4,128)S(1)}, f32[128,4,32,128]{0,3,2,1:T(8,128)S(1)}) fusion(pred[128,32,128]{0,2,1:T(8,128)(4,1)S(1)} %compare_and_fusion.3, f32[128]{0:T(128)S(1)} %get-tuple-element.179, f32[32,128]{1,0:T(8,128)S(1)} %add_rsqrt_fusion.3, bf16[8,32,128,128]{3,2,1,0:T(8,128)(2,1)} %get-tuple-element.178, s32[]{:T(128)} %get-tuple-element.165, ...), kind=kOutput, calls=%fused_computation.7.clone.1 | convolution fusion | flops 545259008 | bytes 10112512 | tf_op jit(solution)/shard_map/while/body/eval_jaxpr/qhl,ckl->qhck/dot_general | solution.py:108
  147.0 2.1 fusion.46
  149.1 4.5 %fusion.47 = bf16[8,128,4,128]{3,1,0,2:T(8,128)(2,1)S(1)} fusion(bf16[8,128,4,128]{3,1,0,2:T(8,128)(2,1)S(1)} %get-tuple-element.166, s32[]{:T(128)} %get-tuple-element.165, f32[128,4,32,128]{0,3,2,1:T(8,128)S(1)} %get-tuple-element.155, f32[128,4]{0,1:T(4,128)S(1)} %fusion.46, f32[128,4]{0,1:T(4,128)S(1)} %get-tuple-element.156, ...), kind=kOutput, calls=%fused_computation.16.clone.1 | convolution fusion | flops 549519360 | bytes 10097664 | tf_op jit(solution)/shard_map/while/body/eval_jaxpr/qhck,ckl->qhl/dot_general | solution.py:123
  156.3 0.8 compare_and_fusion.3
  157.1 1.8 multiply_reduce_fusion.2
  159.0 2.8 %fusion.45 = (f32[128,4]{0,1:T(4,128)S(1)}, f32[128,4,32,128]{0,3,2,1:T(8,128)S(1)}) fusion(pred[128,32,128]{0,2,1:T(8,128)(4,1)S(1)} %compare_and_fusion.3, f32[128]{0:T(128)S(1)} %get-tuple-element.179, f32[32,128]{1,0:T(8,128)S(1)} %add_rsqrt_fusion.3, bf16[8,32,128,128]{3,2,1,0:T(8,128)(2,1)} %get-tuple-element.178, s32[]{:T(128)} %get-tuple-element.165, ...), kind=kOutput, calls=%fused_computation.7.clone.1 | convolution fusion | flops 545259008 | bytes 10112512 | tf_op jit(solution)/shard_map/while/body/eval_jaxpr/qhl,ckl->qhck/dot_general | solution.py:108
  161.8 2.1 fusion.46
  163.8 4.5 %fusion.47 = bf16[8,128,4,128]{3,1,0,2:T(8,128)(2,1)S(1)} fusion(bf16[8,128,4,128]{3,1,0,2:T(8,128)(2,1)S(1)} %get-tuple-element.166, s32[]{:T(128)} %get-tuple-element.165, f32[128,4,32,128]{0,3,2,1:T(8,128)S(1)} %get-tuple-element.155, f32[128,4]{0,1:T(4,128)S(1)} %fusion.46, f32[128,4]{0,1:T(4,128)S(1)} %get-tuple-element.156, ...), kind=kOutput, calls=%fused_computation.16.clone.1 | convolution fusion | flops 549519360 | bytes 10097664 | tf_op jit(solution)/shard_map/while/body/eval_jaxpr/qhck,ckl->qhl/dot_general | solution.py:123
  171.1 0.8 compare_and_fusion.3
  171.9 1.8 multiply_reduce_fusion.2
  173.7 2.8 %fusion.45 = (f32[128,4]{0,1:T(4,128)S(1)}, f32[128,4,32,128]{0,3,2,1:T(8,128)S(1)}) fusion(pred[128,32,128]{0,2,1:T(8,128)(4,1)S(1)} %compare_and_fusion.3, f32[128]{0:T(128)S(1)} %get-tuple-element.179, f32[32,128]{1,0:T(8,128)S(1)} %add_rsqrt_fusion.3, bf16[8,32,128,128]{3,2,1,0:T(8,128)(2,1)} %get-tuple-element.178, s32[]{:T(128)} %get-tuple-element.165, ...), kind=kOutput, calls=%fused_computation.7.clone.1 | convolution fusion | flops 545259008 | bytes 10112512 | tf_op jit(solution)/shard_map/while/body/eval_jaxpr/qhl,ckl->qhck/dot_general | solution.py:108
  176.5 2.1 fusion.46
  178.6 4.5 %fusion.47 = bf16[8,128,4,128]{3,1,0,2:T(8,128)(2,1)S(1)} fusion(bf16[8,128,4,128]{3,1,0,2:T(8,128)(2,1)S(1)} %get-tuple-element.166, s32[]{:T(128)} %get-tuple-element.165, f32[128,4,32,128]{0,3,2,1:T(8,128)S(1)} %get-tuple-element.155, f32[128,4]{0,1:T(4,128)S(1)} %fusion.46, f32[128,4]{0,1:T(4,128)S(1)} %get-tuple-element.156, ...), kind=kOutput, calls=%fused_computation.16.clone.1 | convolution fusion | flops 549519360 | bytes 10097664 | tf_op jit(solution)/shard_map/while/body/eval_jaxpr/qhck,ckl->qhl/dot_general | solution.py:123
  183.6 2.1 convert_bitcast_fusion.1
  185.7 0.8 dynamic_slice.19
  186.5 30.3 %reduce-scatter.2.cloned.1.call-done = bf16[256,1024]{0,1:T(8,128)(2,1)} async-done(((bf16[1024,1024]{0,1:T(8,128)(2,1)}), bf16[256,1024]{0,1:T(8,128)(2,1)}) %reduce-scatter.2.cloned.1.call-update) | async-done | bytes 524304 | tf_op jit(solution)/shard_map/reduce_scatter | solution.py:21
  216.8 1.3 fusion.24
  218.1 6.0 %psum.7 = f32[1024]{0:T(1024)S(1)} all-reduce(f32[1024]{0:T(1024)S(1)} %fusion.24), channel_id=1, replica_groups=mesh['kv'=8,'tp'=4] {'tp'}, use_global_device_ids=true, to_apply=%region_13.14 | all-reduce | flops 1024 | bytes 8192 | tf_op jit(solution)/shard_map/psum | solution.py:146
  224.1 2.0 fusion.27
  (96 shorter events, 25.6 us)
Async XLA Ops:
  6.5 35.8 %copy-start = (bf16[1024,512]{1,0:T(8,128)(2,1)S(1)}, bf16[1024,512]{1,0:T(8,128)(2,1)}, u32[]{:S(2)}) copy-start(bf16[1024,512]{1,0:T(8,128)(2,1)} %param.12) | copy-start | bytes 3145732
  6.5 26.4 %all-gather.2.cloned.1.call-start = ((), (), s32[]{:S(2)}) async-start(), calls=%async_computation.3 | async-start | bytes 2621440 | tf_op jit(solution)/shard_map/all_gather | solution.py:15
  10.4 8.0 %all-to-all-start = ((s32[8,1,2]{2,1,0:T(1,128)}), s32[8,1,2]{2,1,0:T(1,128)S(1)}, u32[]{:S(2)}, u32[]{:S(2)}) async-start(s32[8,1,2]{2,1,0:T(1,128)} %bitcast.27), calls=%async_computation | async-start | bytes 8192 | tf_op jit(solution)/shard_map/all_to_all | solution.py:87
  36.8 18.6 %all-to-all-start.1 = ((bf16[8,2,128,128]{3,2,1,0:T(8,128)(2,1)}), bf16[8,2,128,128]{3,2,1,0:T(8,128)(2,1)}, u32[]{:S(2)}, u32[]{:S(2)}) async-start(bf16[8,2,128,128]{3,2,1,0:T(8,128)(2,1)} %broadcast_select_fusion), calls=%async_computation.1 | async-start | bytes 1048576 | tf_op jit(solution)/shard_map/all_to_all | solution.py:90
  42.3 6.9 %copy-start.4 = (f32[128]{0:T(128)S(1)}, f32[128]{0:T(128)}, u32[]{:S(2)}) copy-start(f32[128]{0:T(128)} %param.14) | copy-start | bytes 1540
  42.3 174.5 %reduce-scatter.2.cloned.1.call-start = ((), (), s32[]{:S(2)}) async-start(), calls=%async_computation.4 | async-start | bytes 2621440 | tf_op jit(solution)/shard_map/reduce_scatter | solution.py:21
  56.6 8.3 %copy-start.1 = (bf16[8,128,4,128]{3,1,0,2:T(8,128)(2,1)S(1)}, bf16[8,128,4,128]{3,1,0,2:T(8,128)(2,1)}, u32[]{:S(2)}) copy-start(bf16[8,128,4,128]{3,1,0,2:T(8,128)(2,1)} %custom-call.6) | copy-start | bytes 3145732
  56.6 8.3 %copy-start.5 = (f32[128]{0:T(128)S(1)}, f32[128]{0:T(128)}, u32[]{:S(2)}) copy-start(f32[128]{0:T(128)} %param.15) | copy-start | bytes 1540
  64.9 118.2 %copy-start.3 = (bf16[4,128,64]{1,2,0:T(8,128)(2,1)S(1)}, bf16[4,128,64]{1,2,0:T(8,128)(2,1)}, u32[]{:S(2)}) copy-start(bf16[4,128,64]{1,2,0:T(8,128)(2,1)} %param.16) | copy-start | bytes 196612
  64.9 118.7 %copy-start.2 = (bf16[256,1024]{1,0:T(8,128)(2,1)S(1)}, bf16[256,1024]{1,0:T(8,128)(2,1)}, u32[]{:S(2)}) copy-start(bf16[256,1024]{1,0:T(8,128)(2,1)} %param.17) | copy-start | bytes 1572868
Sparse Core Ops, SparseCore 0:
  8.9 24.0 all-gather.1
  185.9 30.9 reduce-scatter.1
where the time goes:
time: 237 us; the launch traced here: 233 us
  matrix products  66 us (28%)
  other arithmetic  65.6 us (28%)
  waiting for transfers between devices  49.9 us (21%)
  local copies, waits for them, and re-layouts  20.4 us (9%)
  between operations  13.6 us (6%)
  starting transfers between devices  10.9 us (5%)
  blocking collectives  5.96 us (3%)
    dot_general x8, matrix products, attend(): jnp.einsum('qhck,ckl->qhl', weights, picked_values, preferred_element_typ...  35.9 us
    reduce_scatter x1, waiting for transfers between devices, own_rows(): lax.psum_scatter(everything.astype(jnp.bfloat16), axis, scatter_dimension...  30.3 us
    dot_general x8, matrix products, attend(): jnp.einsum('qhl,ckl->qhck', query_block, picked_keys, preferred_element_t...  22.3 us
    reduce_sum x8, other arithmetic, attend(): jnp.sum(exp_scores, axis=(2, 3), keepdims=True)  16.7 us
    reduce_sum x8, other arithmetic, rms_scale(): mean_sq = jnp.mean(widened * widened, axis=-1, keepdims=True)  14.7 us
    all_gather x1, waiting for transfers between devices, taken_in(): lax.all_gather(part, axis, axis=dim, tiled=True)  14.2 us
    gather x1, local copies, waits for them, and re-layouts, on_device(): selected = block_pool[where_from]  8.33 us
    and x8, other arithmetic, attend(): (chosen_row[:, None] >= 0)[None]  6.28 us
  transfers between devices with their start and end apart: 4, of which 3 were waited for; matrix products, arithmetic and copies ran while one was open for 7% of the time, Pallas kernels for 0%

commit v1 on v0

--- a/solution.py
+++ b/solution.py
@@ -1,6 +1,10 @@
+import functools
+
 import jax
 import jax.numpy as jnp
 from jax import lax
+from jax.experimental import pallas as pl
+from jax.experimental.pallas import tpu as pltpu
 from jax.sharding import PartitionSpec as P
 
 BLOCK = 128
@@ -26,6 +30,62 @@
     widened = values.astype(jnp.float32)
     mean_sq = jnp.mean(widened * widened, axis=-1, keepdims=True)
     return (widened * lax.rsqrt(mean_sq + epsilon) * gain_row).astype(jnp.bfloat16)
+
+
+def norm_keys(pool_ref, gain_ref, kn_ref, vx_ref, rows):
+    lat = pool_ref[rows, :]
+    kn_ref[rows, :] = rms_scale(lat, gain_ref[...])
+    vx_ref[rows, 0:lat.shape[1]] = lat
+    vx_ref[rows, lat.shape[1] :] = jnp.ones_like(lat)
+
+
+def attend_block(b, own_pairs, q_ref, kn_ref, vx_ref, bias_ref, p_ref, vu_ref):
+    width = kn_ref.shape[1]
+    heads = q_ref.shape[1] // width
+    pairs = kn_ref.shape[0] // (2 * BLOCK)
+    rows = pl.ds(pl.multiple_of(b * BLOCK, BLOCK), BLOCK)
+    q = jnp.concatenate([q_ref[rows, h * width : (h + 1) * width] for h in range(heads)], axis=0)
+    shape = (heads * BLOCK, 2 * BLOCK)
+    row_pos = lax.broadcasted_iota(jnp.int32, shape, 0) % BLOCK + b * BLOCK
+    col_pos = lax.broadcasted_iota(jnp.int32, shape, 1)
+    for i in range(pairs):
+        cols = slice(i * 2 * BLOCK, (i + 1) * 2 * BLOCK)
+        s = lax.dot_general(
+            q, kn_ref[cols, :], (((1,), (1,)), ((), ())), preferred_element_type=jnp.float32
+        )
+        s = s + bias_ref[b, :, cols]
+        if i < own_pairs:
+            s = jnp.where(col_pos + i * 2 * BLOCK <= row_pos, s, masked_score)
+        p_ref[:, cols] = jnp.exp2(s).astype(jnp.bfloat16)
+    acc = jnp.dot(p_ref[...], vx_ref[...], preferred_element_type=jnp.float32)
+    att = (acc[:, :width] / acc[:, width:]).astype(jnp.bfloat16)
+    out = []
+    for h in range(0, heads, 2):
+        two = jnp.concatenate(
+            [att[h * BLOCK : (h + 1) * BLOCK], att[(h + 1) * BLOCK : (h + 2) * BLOCK]], axis=1
+        )
+        out.append(jnp.dot(two, vu_ref[h // 2], preferred_element_type=jnp.float32))
+    return jnp.concatenate(out, axis=1).astype(jnp.bfloat16)
+
+
+def attention_kernel(own_pairs, q_ref, pool_ref, bias_ref, gain_ref, vu_ref, o_ref, kn_ref, vx_ref, p_ref):
+    @pl.loop(0, pool_ref.shape[0] // (2 * BLOCK))
+    def _(i):
+        norm_keys(pool_ref, gain_ref, kn_ref, vx_ref, pl.ds(pl.multiple_of(i * 2 * BLOCK, 2 * BLOCK), 2 * BLOCK))
+
+    @pl.loop(0, q_ref.shape[0] // BLOCK)
+    def _(b):
+        o_ref[pl.ds(pl.multiple_of(b * BLOCK, BLOCK), BLOCK), :] = attend_block(
+            b, own_pairs, q_ref, kn_ref, vx_ref, bias_ref, p_ref, vu_ref
+        )
+
+
+def paired_up(value_up):
+    heads, width, vdim = value_up.shape
+    pairs = value_up.reshape(heads // 2, 2, width, vdim)
+    first = jnp.pad(pairs[:, 0], ((0, 0), (0, 0), (0, vdim)))
+    second = jnp.pad(pairs[:, 1], ((0, 0), (0, 0), (vdim, 0)))
+    return jnp.concatenate([first, second], axis=1)
 
 
 def on_device(
@@ -59,9 +119,10 @@
     query_zero = jnp.zeros((tok_rows, head_cols), jnp.float32)
     latent_zero = jnp.zeros((tok_rows, lat_width), jnp.float32)
     query_acc, latent_acc = taken_in(tokens, "tp", 1, project, (query_zero, latent_zero))
+    scaled_gain = query_gain * (lat_width**-0.5 * 1.4426950408889634)
     queries = rms_scale(
-        query_acc.astype(jnp.bfloat16).reshape(tok_rows, local_heads, lat_width), query_gain
-    )
+        query_acc.astype(jnp.bfloat16).reshape(tok_rows, local_heads, lat_width), scaled_gain
+    ).reshape(tok_rows, head_cols)
     latent = latent_acc.astype(jnp.bfloat16)
     latent_blocks = latent.reshape(blocks_dev, block_size, lat_width)
     clamped = jnp.maximum(chosen, 0)
@@ -91,44 +152,25 @@
     block_pool = jnp.concatenate(
         [latent_blocks, arrived.reshape(owners * PER_OWNER, block_size, lat_width)], axis=0
     )
-    slot_of = jnp.sum(jnp.where(wanted[owner_of] == index_in[:, :, None], slot_ids, 0), axis=2)
-    where_from = jnp.where(
-        owner_of == my_owner, index_in, blocks_dev + owner_of * PER_OWNER + slot_of
-    )
-    selected = block_pool[where_from]
-    score_scale = lat_width ** (-0.5)
-    offsets = jnp.arange(block_size, dtype=jnp.int32)
-    query_blocks = queries.reshape(blocks_dev, block_size, local_heads, lat_width)
-    block_starts = my_owner * tok_rows + jnp.arange(blocks_dev, dtype=jnp.int32) * block_size
-
-    def attend(packed):
-        query_block, picked_values, chosen_row, start_pos = packed
-        picked_keys = rms_scale(picked_values, key_gain)
-        scores = (
-            jnp.einsum(
-                "qhl,ckl->qhck", query_block, picked_keys, preferred_element_type=jnp.float32
-            )
-            * score_scale
-        )
-        key_pos = jnp.maximum(chosen_row, 0)[:, None] * block_size + offsets[None, :]
-        query_pos = start_pos + offsets
-        allowed = (chosen_row[:, None] >= 0)[None] & (key_pos[None] <= query_pos[:, None, None])
-        allowed = allowed[:, None]
-        scores = jnp.where(allowed, scores, masked_score)
-        row_max = jnp.max(scores, axis=(2, 3), keepdims=True)
-        exp_scores = jnp.where(allowed, jnp.exp(scores - row_max), 0.0)
-        weights = (exp_scores / jnp.sum(exp_scores, axis=(2, 3), keepdims=True)).astype(
-            jnp.bfloat16
-        )
-        attended = jnp.einsum(
-            "qhck,ckl->qhl", weights, picked_values, preferred_element_type=jnp.float32
-        )
-        return attended.astype(jnp.bfloat16)
-
-    attended = lax.map(attend, (query_blocks, selected, chosen, block_starts))
-    attended = attended.reshape(tok_rows, local_heads, lat_width)
-    heads_out = jnp.einsum("thl,hlv->thv", attended, value_up, preferred_element_type=jnp.float32)
-    heads_out = heads_out.astype(jnp.bfloat16).reshape(tok_rows, local_heads * value_up.shape[2])
+    own_id = my_owner * blocks_dev + local_ids
+    far_id = jnp.where(wanted >= 0, wanted + owner_ids[:, None] * blocks_dev, -2).reshape(-1)
+    slot_block = jnp.concatenate([own_id, far_id])
+    hit = jnp.any(chosen[:, :, None] == slot_block[None, None, :], axis=1)
+    bias = jnp.repeat(jnp.where(hit, 0.0, masked_score), block_size, axis=1)[:, None, :]
+    pool = block_pool.reshape(-1, lat_width)
+    vdim = value_up.shape[2]
+    heads_out = pl.pallas_call(
+        functools.partial(attention_kernel, blocks_dev // 2),
+        out_shape=jax.ShapeDtypeStruct((tok_rows, local_heads * vdim), jnp.bfloat16),
+        in_specs=[pl.BlockSpec(memory_space=pltpu.VMEM)] * 5,
+        out_specs=pl.BlockSpec(memory_space=pltpu.VMEM),
+        scratch_shapes=[
+            pltpu.VMEM(pool.shape, jnp.bfloat16),
+            pltpu.VMEM((pool.shape[0], 2 * lat_width), jnp.bfloat16),
+            pltpu.VMEM((local_heads * block_size, pool.shape[0]), jnp.bfloat16),
+        ],
+        compiler_params=pltpu.CompilerParams(vmem_limit_bytes=60 << 20),
+    )(queries, pool, bias, key_gain[None, :], paired_up(value_up))
     model_width = out_weight.shape[1]
     tp_count = lax.axis_size("tp")
     feature_rows = model_width // tp_count

time: 237 us -> 133 us (0.56)
  matrix products: 66 us -> 8.32 us
  other arithmetic: 65.6 us -> 16.5 us
  Pallas kernels: 0 us -> 20.3 us
  local copies, waits for them, and re-layouts: 20.4 us -> 8.45 us
  waiting for transfers between devices: 49.9 us -> 46.8 us
    dot_general x17 -> x0, matrix products: 58.7 us -> none  [the longest x8 35.9 us: attend(): jnp.einsum('qhck,ckl->qhl', weights, picked_values, preferred_element_typ...]
    pallas_call x0 -> x1, Pallas kernels: none -> 20.3 us  [on_device(): pl.pallas_call(functools.partial(attention_kernel, blocks_dev // 2), out_...]
    reduce_sum x9 -> x0, other arithmetic: 17 us -> none  [the longest x8 16.7 us: attend(): jnp.sum(exp_scores, axis=(2, 3), keepdims=True)]
    reduce_sum x8 -> x1, other arithmetic: 14.7 us -> 1.95 us  [rms_scale(): mean_sq = jnp.mean(widened * widened, axis=-1, keepdims=True)]
    gather x2 -> x0, local copies, waits for them, and re-layouts: 9.73 us -> none  [the longest x1 8.33 us: on_device(): selected = block_pool[where_from]]
    and x8 -> x0, other arithmetic: 6.28 us -> none  [attend(): (chosen_row[:, None] >= 0)[None]]
    add x17 -> x1, other arithmetic: 5.77 us -> 0.01 us  [on_device(): own_id = my_owner * blocks_dev + local_ids]
    ge x8 -> x0, other arithmetic: 5.57 us -> none  [attend(): chosen_row[:, None] >= 0]
  transfers between devices with their start and end apart: 4 -> 4, of which waited for: 3 -> 3; matrix products, arithmetic and copies ran while one was open for 7% -> 14% of each run, Pallas kernels for 0% -> 0%
where the time goes in v1:
time: 133 us; the launch traced here: 131 us
  waiting for transfers between devices  46.8 us (35%)
  Pallas kernels  20.3 us (15%)
  other arithmetic  16.5 us (12%)
  between operations  13.5 us (10%)
  starting transfers between devices  10.9 us (8%)
  local copies, waits for them, and re-layouts  8.45 us (6%)
  matrix products  8.32 us (6%)
  blocking collectives  5.95 us (4%)
    reduce_scatter x1, waiting for transfers between devices, own_rows(): lax.psum_scatter(everything.astype(jnp.bfloat16), axis, scatter_dimension...  30.3 us
    pallas_call x1, Pallas kernels, on_device(): pl.pallas_call(functools.partial(attention_kernel, blocks_dev // 2), out_...  20.3 us
    all_gather x1, waiting for transfers between devices, taken_in(): lax.all_gather(part, axis, axis=dim, tiled=True)  13.2 us
    psum x1, blocking collectives, on_device(): squares = lax.psum(jnp.sum(summed * summed, axis=1), 'tp')  5.95 us
    all_to_all x1, starting transfers between devices, on_device(): lax.all_to_all(wanted, 'kv', split_axis=0, concat_axis=0, tiled=True)  5.44 us
    all_to_all x1, starting transfers between devices, on_device(): lax.all_to_all(served, 'kv', split_axis=0, concat_axis=0, tiled=True)  5.44 us
    dot_general x1, matrix products, columns(): lax.dot_general(weight_cols, heads_out, (((0,), (1,)), ((), ())), preferr...  3.11 us
    dot_general x1, matrix products, project(): jnp.dot(shard_piece, query_rows, preferred_element_type=jnp.float32)  2.92 us
  transfers between devices with their start and end apart: 4, of which 3 were waited for; matrix products, arithmetic and copies ran while one was open for 14% of the time, Pallas kernels for 0%

profile of v1, /device:TPU:29, one launch (start us, length us, event | category | flops | bytes accessed | tf_op | source)
XLA Modules:
  0.0 130.7 jit_solution(11319927966567861654)
XLA Ops:
  6.5 0.0 copy-start
  6.5 0.0 all-gather.2.cloned.1.call-start
  6.5 0.7 all-gather.2.cloned.1.call-update
  7.3 0.7 add_select_fusion.1
  8.0 0.7 broadcast_compare_fusion.1
  8.7 0.1 reshape.179
  8.7 0.1 ge.30
  8.8 0.1 eq.69
  8.9 0.2 and_reduce_fusion
  9.2 0.2 reduce_window_sum.11
  9.3 0.1 fusion.11
  9.5 0.2 select_reduce_fusion
  9.6 0.7 copy.45
  10.3 5.4 %all-to-all-start = ((s32[8,1,2]{2,1,0:T(1,128)}), s32[8,1,2]{2,1,0:T(1,128)S(1)}, u32[]{:S(2)}, u32[]{:S(2)}) async-start(s32[8,1,2]{2,1,0:T(1,128)} %copy.45), calls=%async_computation | async-start | bytes 8192 | tf_op jit(solution)/shard_map/all_to_all | solution.py:148
  15.7 0.1 copy.48
  15.8 0.1 select_n.58
  15.9 0.8 fusion.13
  16.7 0.1 copy.52
  16.8 0.1 copy.53
  17.0 0.1 pad_add_fusion
  17.0 1.0 compare_reduce_fusion
  18.0 0.7 broadcast_multiply_fusion
  18.7 0.7 fusion.8.vu_ref
  19.4 0.0 all-to-all-done
  19.4 0.1 reshape.185
  19.5 0.1 copy.46
  19.6 0.1 copy.47
  19.7 13.2 %all-gather.2.cloned.1.call-done = bf16[1024,1024]{1,0:T(8,128)(2,1)} async-done(((bf16[1024,256]{1,0:T(8,128)(2,1)}), bf16[1024,1024]{1,0:T(8,128)(2,1)}) %all-gather.2.cloned.1.call-update) | async-done | bytes 2097168 | tf_op jit(solution)/shard_map/all_gather | solution.py:19
  33.0 2.3 %convolution_convert_fusion.1 = bf16[1024,128]{1,0:T(8,128)(2,1)S(1)} fusion(bf16[1024,1024]{1,0:T(8,128)(2,1)} %all-gather.2.cloned.1.call-done, bf16[1024,128]{1,0:T(8,128)(2,1)} %param.11), kind=kOutput, calls=%fused_computation.9 | convolution fusion | flops 268566528 | bytes 2621440 | tf_op jit(solution)/shard_map/dot_general | solution.py:116
  35.3 0.0 copy-start.1
  35.3 1.4 %gather_fusion = bf16[16,128,128]{2,1,0:T(8,128)(2,1)} fusion(bf16[8,128,128]{2,1,0:T(8,128)(2,1)S(1)} %bitcast.28, s32[1024]{0:T(1024)S(1)} %pad_clamp_fusion), kind=kCustom, calls=%fused_computation | custom fusion | bytes 1048640 | tf_op jit(solution)/shard_map/gather | solution.py:149
  36.7 2.0 %broadcast_select_fusion = bf16[8,2,128,128]{3,2,1,0:T(8,128)(2,1)} fusion(bf16[8,2,128,128]{3,2,1,0:T(8,128)(2,1)} %bitcast.31, pred[8,2]{1,0:T(8,128)(4,1)S(1)} %copy.47), kind=kLoop, calls=%fused_computation.16 | loop fusion | flops 262144 | bytes 1048592 | tf_op jit(solution)/shard_map/jit(_where)/select_n | solution.py:150
  38.6 5.4 %all-to-all-start.1 = ((bf16[8,2,128,128]{3,2,1,0:T(8,128)(2,1)}), bf16[8,2,128,128]{3,2,1,0:T(8,128)(2,1)}, u32[]{:S(2)}, u32[]{:S(2)}) async-start(bf16[8,2,128,128]{3,2,1,0:T(8,128)(2,1)} %broadcast_select_fusion), calls=%async_computation.1 | async-start | bytes 1048576 | tf_op jit(solution)/shard_map/all_to_all | solution.py:151
  44.1 0.0 reduce-scatter.2.cloned.1.call-start
  44.1 0.0 copy-done
  44.1 0.0 copy-done.1
  44.1 2.9 %convert_multiply_fusion.1 = (f32[1024,512]{1,0:T(8,128)}, bf16[1024,512]{1,0:T(8,128)(2,1)}) fusion(bf16[1024,1024]{1,0:T(8,128)(2,1)S(1)} %copy-done.1, bf16[1024,512]{1,0:T(8,128)(2,1)S(1)} %copy-done), kind=kOutput, calls=%fused_computation.2 | convolution fusion | flops 1075314688 | bytes 6291456 | tf_op jit(solution)/shard_map/dot_general | solution.py:115
  47.0 1.9 %mul.73 = f32[1024,4,128]{2,1,0:T(4,128)S(1)} reshape(f32[1024,512]{1,0:T(8,128)} %get-tuple-element.11) | data formatting | bytes 4194304 | tf_op jit(solution)/shard_map/mul | solution.py:31
  49.0 1.9 %reduce_sum.27 = f32[1024,4]{1,0:T(8,128)} reduce(f32[1024,4,128]{2,1,0:T(4,128)S(1)} %mul.73, f32[]{:T(128)} %constant.34.clone.1), dimensions={2}, to_apply=%region_0.0 | reduce | flops 520192 | bytes 2113540 | tf_op jit(solution)/shard_map/reduce_sum | solution.py:31
  50.9 0.0 copy-start.2
  50.9 1.2 add_rsqrt_fusion
  52.1 1.2 mul.74
  53.4 0.0 copy-done.2
  53.4 1.4 %fusion.1.q_ref = bf16[1024,512]{1,0:T(8,128)(2,1)} fusion(bf16[1024,512]{1,0:T(8,128)(2,1)S(1)} %copy-done.2, f32[128,8,4,128]{3,2,1,0:T(4,128)S(1)} %bitcast.27, f32[512]{0:T(512)S(1)} %broadcast_bitcast_fusion), kind=kLoop, calls=%fused_computation.4 | loop fusion | flops 2097152 | bytes 4196352 | tf_op jit(solution)/shard_map/convert_element_type | solution.py:32
  54.8 2.5 %all-to-all-done.1 = bf16[8,2,128,128]{3,2,1,0:T(8,128)(2,1)} async-done(((bf16[8,2,128,128]{3,2,1,0:T(8,128)(2,1)}), bf16[8,2,128,128]{3,2,1,0:T(8,128)(2,1)}, u32[]{:S(2)}, u32[]{:S(2)}) %all-to-all-start.1) | async-done | bytes 524320 | tf_op jit(solution)/shard_map/all_to_all | solution.py:151
  57.3 0.0 copy-start.3
  57.3 2.1 %pad_maximum_fusion = bf16[24,128,128]{2,1,0:T(8,128)(2,1)} fusion(bf16[16,128,128]{2,1,0:T(8,128)(2,1)} %bitcast.5, bf16[8,128,128]{2,1,0:T(8,128)(2,1)S(1)} %bitcast.29), kind=kLoop, calls=%fused_computation.13 | loop fusion | flops 393216 | bytes 1572864 | tf_op jit(solution)/shard_map/concatenate | solution.py:152
  59.4 0.7 broadcast_in_dim.68
  60.1 20.3 %shard_map.91 = bf16[1024,256]{1,0:T(8,128)(2,1)} custom-call(bf16[1024,512]{1,0:T(8,128)(2,1)} %fusion.1.q_ref, bf16[3072,128]{1,0:T(8,128)(2,1)} %bitcast.30, f32[8,1,3072]{2,1,0:T(1,128)} %bitcast.32, f32[1,128]{1,0:T(1,128)} %bitcast.37, bf16[2,256,128]{2,1,0:T(8,128)(2,1)} %fusion.8.vu_ref), custom_call_target="tpu_custom_call" | custom-call | tf_op jit(solution)/shard_map/pallas_call | solution.py:162
  80.3 0.0 copy-done.3
  80.3 3.1 %convert_bitcast_fusion = bf16[1024,1024]{0,1:T(8,128)(2,1)} fusion(bf16[1024,256]{1,0:T(8,128)(2,1)} %shard_map.91, bf16[256,1024]{1,0:T(8,128)(2,1)S(1)} %copy-done.3), kind=kOutput, calls=%fused_computation.5 | convolution fusion | flops 537919488 | bytes 3145728 | tf_op jit(solution)/shard_map/dot_general | solution.py:183
  83.4 0.0 reduce-scatter.2.cloned.1.call-update
  83.5 0.8 dynamic_slice.3
  84.2 30.3 %reduce-scatter.2.cloned.1.call-done = bf16[256,1024]{0,1:T(8,128)(2,1)} async-done(((bf16[1024,1024]{0,1:T(8,128)(2,1)}), bf16[256,1024]{0,1:T(8,128)(2,1)}) %reduce-scatter.2.cloned.1.call-update) | async-done | bytes 524304 | tf_op jit(solution)/shard_map/reduce_scatter | solution.py:25
  114.6 1.3 fusion.2
  115.8 6.0 %psum.7 = f32[1024]{0:T(1024)S(1)} all-reduce(f32[1024]{0:T(1024)S(1)} %fusion.2), channel_id=1, replica_groups=mesh['kv'=8,'tp'=4] {'tp'}, use_global_device_ids=true, to_apply=%region_8.9 | all-reduce | flops 1024 | bytes 8192 | tf_op jit(solution)/shard_map/psum | solution.py:188
  121.8 2.0 %fusion.5 = bf16[1024,256]{1,0:T(8,128)(2,1)} fusion(bf16[256,1024]{0,1:T(8,128)(2,1)} %reduce-scatter.2.cloned.1.call-done, f32[256]{0:T(256)S(1)} %dynamic_slice.3, f32[1024]{0:T(1024)S(1)} %add_rsqrt_fusion.1), kind=kLoop, calls=%fused_computation.14 | loop fusion | flops 1048576 | bytes 1053696 | tf_op jit(solution)/shard_map/convert_element_type | solution.py:189
  (13 shorter events, 0.1 us)
Async XLA Ops:
  6.5 37.6 %copy-start = (bf16[1024,512]{1,0:T(8,128)(2,1)S(1)}, bf16[1024,512]{1,0:T(8,128)(2,1)}, u32[]{:S(2)}) copy-start(bf16[1024,512]{1,0:T(8,128)(2,1)} %param.10) | copy-start | bytes 3145732
  6.5 26.4 %all-gather.2.cloned.1.call-start = ((), (), s32[]{:S(2)}) async-start(), calls=%async_computation.3 | async-start | bytes 2621440 | tf_op jit(solution)/shard_map/all_gather | solution.py:19
  10.3 9.1 %all-to-all-start = ((s32[8,1,2]{2,1,0:T(1,128)}), s32[8,1,2]{2,1,0:T(1,128)S(1)}, u32[]{:S(2)}, u32[]{:S(2)}) async-start(s32[8,1,2]{2,1,0:T(1,128)} %copy.45), calls=%async_computation | async-start | bytes 8192 | tf_op jit(solution)/shard_map/all_to_all | solution.py:148
  35.3 8.8 %copy-start.1 = (bf16[1024,1024]{1,0:T(8,128)(2,1)S(1)}, bf16[1024,1024]{1,0:T(8,128)(2,1)}, u32[]{:S(2)}) copy-start(bf16[1024,1024]{1,0:T(8,128)(2,1)} %all-gather.2.cloned.1.call-done) | copy-start | bytes 6291460
  38.6 18.6 %all-to-all-start.1 = ((bf16[8,2,128,128]{3,2,1,0:T(8,128)(2,1)}), bf16[8,2,128,128]{3,2,1,0:T(8,128)(2,1)}, u32[]{:S(2)}, u32[]{:S(2)}) async-start(bf16[8,2,128,128]{3,2,1,0:T(8,128)(2,1)} %broadcast_select_fusion), calls=%async_computation.1 | async-start | bytes 1048576 | tf_op jit(solution)/shard_map/all_to_all | solution.py:151
  44.1 70.5 %reduce-scatter.2.cloned.1.call-start = ((), (), s32[]{:S(2)}) async-start(), calls=%async_computation.4 | async-start | bytes 2621440 | tf_op jit(solution)/shard_map/reduce_scatter | solution.py:25
  50.9 2.5 %copy-start.2 = (bf16[1024,512]{1,0:T(8,128)(2,1)S(1)}, bf16[1024,512]{1,0:T(8,128)(2,1)}, u32[]{:S(2)}) copy-start(bf16[1024,512]{1,0:T(8,128)(2,1)} %get-tuple-element.12) | copy-start | bytes 3145732
  57.3 23.1 %copy-start.3 = (bf16[256,1024]{1,0:T(8,128)(2,1)S(1)}, bf16[256,1024]{1,0:T(8,128)(2,1)}, u32[]{:S(2)}) copy-start(bf16[256,1024]{1,0:T(8,128)(2,1)} %param.15) | copy-start | bytes 1572868
Sparse Core Ops, SparseCore 0:
  8.9 24.0 all-gather.1
  83.6 30.9 reduce-scatter.1

commit v2 on v1

v2 whole, which is shorter than its diff:
```python
import functools

import jax
import jax.numpy as jnp
from jax import lax
from jax.experimental import pallas as pl
from jax.experimental.pallas import tpu as pltpu
from jax.sharding import PartitionSpec as P

BLOCK = 128
PER_OWNER = 2
CHUNKS = 4
LAG = 2
MESH = pl.DeviceIdType.MESH

epsilon = 1e-06
masked_score = -1e30


def rms_scale(values, gain_row):
    widened = values.astype(jnp.float32)
    mean_sq = jnp.mean(widened * widened, axis=-1, keepdims=True)
    return (widened * lax.rsqrt(mean_sq + epsilon) * gain_row).astype(jnp.bfloat16)


def norm_keys(pool_ref, gain_ref, kn_ref, vx_ref, rows):
    lat = pool_ref[rows, :]
    kn_ref[rows, :] = rms_scale(lat, gain_ref[...])
    vx_ref[rows, 0:lat.shape[1]] = lat
    vx_ref[rows, lat.shape[1] :] = jnp.ones_like(lat)


def attend_block(b, own_pairs, q_ref, kn_ref, vx_ref, bias_ref, p_ref, vu_ref):
    width = kn_ref.shape[1]
    heads = q_ref.shape[1] // width
    pairs = kn_ref.shape[0] // (2 * BLOCK)
    rows = pl.ds(pl.multiple_of(b * BLOCK, BLOCK), BLOCK)
    q = jnp.concatenate([q_ref[rows, h * width : (h + 1) * width] for h in range(heads)], axis=0)
    shape = (heads * BLOCK, 2 * BLOCK)
    row_pos = lax.broadcasted_iota(jnp.int32, shape, 0) % BLOCK + b * BLOCK
    col_pos = lax.broadcasted_iota(jnp.int32, shape, 1)
    for i in range(pairs):
        cols = slice(i * 2 * BLOCK, (i + 1) * 2 * BLOCK)
        s = lax.dot_general(
            q, kn_ref[cols, :], (((1,), (1,)), ((), ())), preferred_element_type=jnp.float32
        )
        s = s + bias_ref[pl.ds(b, 1), cols]
        if i < own_pairs:
            s = jnp.where(col_pos + i * 2 * BLOCK <= row_pos, s, masked_score)
        p_ref[:, cols] = jnp.exp2(s).astype(jnp.bfloat16)
    acc = jnp.dot(p_ref[...], vx_ref[...], preferred_element_type=jnp.float32)
    att = (acc[:, :width] / acc[:, width:]).astype(jnp.bfloat16)
    out = []
    for h in range(0, heads, 2):
        two = jnp.concatenate(
            [att[h * BLOCK : (h + 1) * BLOCK], att[(h + 1) * BLOCK : (h + 2) * BLOCK]], axis=1
        )
        out.append(jnp.dot(two, vu_ref[h // 2], preferred_element_type=jnp.float32))
    return jnp.concatenate(out, axis=1).astype(jnp.bfloat16)


def paired_up(value_up):
    heads, width, vdim = value_up.shape
    pairs = value_up.reshape(heads // 2, 2, width, vdim)
    first = jnp.pad(pairs[:, 0], ((0, 0), (0, 0), (0, vdim)))
    second = jnp.pad(pairs[:, 1], ((0, 0), (0, 0), (vdim, 0)))
    return jnp.concatenate([first, second], axis=1)


def picked(table, first, count):
    found, rank = [], jnp.zeros((1, 1), jnp.float32)
    for j in range(count):
        rows = jnp.max(jnp.where(table == first + j, 1.0, 0.0), axis=1, keepdims=True)
        need = jnp.max(rows, axis=0, keepdims=True)
        found.append((rows, need, rank))
        rank = rank + need
    return found


def send(src, dst, sems, where):
    return pltpu.make_async_remote_copy(
        src_ref=src, dst_ref=dst, send_sem=sems[0], recv_sem=sems[1], device_id=where, device_id_type=MESH
    )


def kernel(
    kv_n, tp_n,
    tok_ref, wq_ref, wl_ref, qgain_ref, kgain_ref, vu_ref, w_ref, ogain_ref, chosen_ref,
    o_ref,
    tk_ref, q_ref, pool_ref, bias_ref, chs_ref, out_ref, kn_ref, vx_ref, p_ref,
    ho_ref, wc_ref, proj_ref, ss_ref, rs_ref,
    ch_s, ch_r, ts_s, ts_r, tx_s, tx_r, tr_s, tr_r, b_s, b_r, f_s, f_r,
    hs_s, hs_r, hx_s, hx_r, hr_s, hr_r, w_s, w_r, s_s, s_r,
):
    kv, tp = lax.axis_index("kv"), lax.axis_index("tp")
    core = lax.rem(tp, 2)
    sib = tp + 1 - 2 * core
    far = tp_n // 2 - 1
    toks, feat = tok_ref.shape
    width = wl_ref.shape[1]
    heads = wq_ref.shape[1] // width
    blocks = toks // BLOCK
    cols = o_ref.shape[1]
    crows = toks // CHUNKS

    def at_kv(other):
        return {"kv": other, "tp": tp}

    def at_tp(other):
        return {"kv": kv, "tp": other}

    def across(i, sign):
        return lax.rem(tp + sign * 2 * (i + 1) + tp_n, tp_n)

    barrier = pltpu.get_barrier_semaphore()
    for d in range(1, kv_n):
        pl.semaphore_signal(barrier, inc=1, device_id=at_kv(lax.rem(kv + d, kv_n)), device_id_type=MESH)
    for d in range(1, tp_n):
        pl.semaphore_signal(barrier, inc=1, device_id=at_tp(lax.rem(tp + d, tp_n)), device_id_type=MESH)
    pl.semaphore_wait(barrier, kv_n - 1 + tp_n - 1)

    def rows_of(c, n):
        return pl.ds(pl.multiple_of(c * n, n), n)

    def to_sib(src, buf, c, n, sems):
        return send(src.at[rows_of(c, n)], buf.at[tp, rows_of(c, n)], [s.at[c] for s in sems], at_tp(sib))

    def to_far(src, buf, c, n, i, sems):
        return send(
            src.at[rows_of(c, n)], buf.at[tp, rows_of(c, n)], [s.at[i, c] for s in sems], at_tp(across(i, 1))
        )

    def relay(buf, c, n, i, sems):
        part = buf.at[across(i, -1), rows_of(c, n)]
        return send(part, part, [s.at[i, c] for s in sems], at_tp(sib))

    def from_far(buf, c, n, i, sems):
        part = buf.at[across(i, -1), rows_of(c, n)]
        return send(part, part, [s.at[i, c] for s in sems], at_tp(sib))

    for c in range(CHUNKS):
        for i in range(far):
            to_far(tok_ref, tk_ref, c, crows, i, (tx_s, tx_r)).start()
        to_sib(tok_ref, tk_ref, c, crows, (ts_s, ts_r)).start()

    def ask(d):
        return send(chosen_ref, chs_ref.at[d - 1], (ch_s.at[d - 1], ch_r.at[d - 1]), at_kv(lax.rem(kv - d + kv_n, kv_n)))

    for d in range(1, kv_n):
        ask(d).start()

    tk_ref[tp] = tok_ref[...]
    table = chosen_ref[...]

    def put_bias(slot, hit):
        bias_ref[:, slot * BLOCK : (slot + 1) * BLOCK] = jnp.broadcast_to(
            (1.0 - hit) * masked_score, (blocks, BLOCK)
        )

    for j, (rows, _, _) in enumerate(picked(table, kv * blocks, blocks)):
        put_bias(j, rows)
    for d in range(1, kv_n):
        owner = kv - d
        first = jnp.where(owner >= 0, owner * blocks, -4 * blocks)
        found = picked(table, first, blocks)
        for k in range(PER_OWNER):
            hit = jnp.zeros((blocks, 1), jnp.float32)
            for rows, _, rank in found:
                hit = hit + jnp.where(rank == k, rows, 0.0)
            put_bias(blocks + (d - 1) * PER_OWNER + k, hit)

        @pl.when(owner < 0)
        def _(d=d):
            at = (blocks + (d - 1) * PER_OWNER) * BLOCK
            pool_ref[at : at + PER_OWNER * BLOCK, :] = jnp.zeros((PER_OWNER * BLOCK, width), jnp.bfloat16)

    gain = qgain_ref[...]

    def project(c):
        rows = slice(c * crows, (c + 1) * crows)
        x = jnp.concatenate([tk_ref[t, rows, :] for t in range(tp_n)], axis=1)
        lat = jnp.dot(x, wl_ref[...], preferred_element_type=jnp.float32)
        pool_ref[rows, :] = lat.astype(jnp.bfloat16)
        qs = jnp.dot(x, wq_ref[...], preferred_element_type=jnp.float32).astype(jnp.bfloat16)
        for h in range(heads):
            hc = slice(h * width, (h + 1) * width)
            q_ref[rows, hc] = rms_scale(qs[:, hc], gain)

    def arrive(c):
        to_sib(tok_ref, tk_ref, c, crows, (ts_s, ts_r)).wait()
        for i in range(far):
            relay(tk_ref, c, crows, i, (tr_s, tr_r)).wait()
            to_far(tok_ref, tk_ref, c, crows, i, (tx_s, tx_r)).wait_send()
        project(c)

    for c in range(CHUNKS):
        for i in range(far):
            from_far(tk_ref, c, crows, i, (tx_s, tx_r)).wait_recv()
            relay(tk_ref, c, crows, i, (tr_s, tr_r)).start()
        if c:
            arrive(c - 1)
    arrive(CHUNKS - 1)

    def weight(d):
        other = lax.rem(tp + d, tp_n)
        part = w_ref.at[:, pl.ds(pl.multiple_of(other * cols, cols), cols)]
        return send(part, wc_ref.at[tp], (w_s.at[d - 1], w_r.at[d - 1]), at_tp(other))

    def slot_rows(d, c):
        return pl.ds(pl.multiple_of((blocks + (d - 1) * PER_OWNER + c) * BLOCK, BLOCK), BLOCK)

    def give(d):
        return send(
            out_ref.at[d - 1], pool_ref.at[slot_rows(d, core)], (b_s.at[d - 1], b_r.at[d - 1]), at_kv(lax.rem(kv + d, kv_n))
        )

    def forward(d):
        part = pool_ref.at[slot_rows(d, core)]
        return send(part, part, (f_s.at[d - 1], f_r.at[d - 1]), at_tp(sib))

    mine = core.astype(jnp.float32)
    for d in range(1, kv_n):
        ask(d).wait()

        @pl.when(kv + d < kv_n)
        def _(d=d):
            total = jnp.zeros((BLOCK, width), jnp.float32)
            for j, (_, need, rank) in enumerate(picked(chs_ref[d - 1], kv * blocks, blocks)):
                share = jnp.where(rank == mine, need, 0.0)
                total = total + share * pool_ref[j * BLOCK : (j + 1) * BLOCK, :].astype(jnp.float32)
            out_ref[d - 1] = total.astype(jnp.bfloat16)
            give(d).start()

    for d in range(1, tp_n):
        weight(d).start()

    def norm(i):
        rows = pl.ds(pl.multiple_of(i * 2 * BLOCK, 2 * BLOCK), 2 * BLOCK)
        norm_keys(pool_ref, kgain_ref, kn_ref, vx_ref, rows)

    pl.loop(0, blocks // 2)(norm)
    wc_ref[tp] = w_ref[:, pl.ds(pl.multiple_of(tp * cols, cols), cols)]

    for d in range(1, kv_n):

        @pl.when(kv - d >= 0)
        def _(d=d):
            give(d).wait_recv()
            forward(d).start()

    for d in range(1, kv_n):

        @pl.when(kv - d >= 0)
        def _(d=d):
            forward(d).wait()

        norm(jnp.int32(blocks // 2 + d - 1))

    for d in range(1, kv_n):

        @pl.when(kv + d < kv_n)
        def _(d=d):
            give(d).wait_send()

    def hand_on(b):
        for i in range(far):
            from_far(ho_ref, b, BLOCK, i, (hx_s, hx_r)).wait_recv()
            relay(ho_ref, b, BLOCK, i, (hr_s, hr_r)).start()

    @pl.loop(0, blocks)
    def _(b):
        ho_ref[tp, rows_of(b, BLOCK), :] = attend_block(
            b, blocks // 2, q_ref, kn_ref, vx_ref, bias_ref, p_ref, vu_ref
        )
        for i in range(far):
            to_far(ho_ref.at[tp], ho_ref, b, BLOCK, i, (hx_s, hx_r)).start()
        to_sib(ho_ref.at[tp], ho_ref, b, BLOCK, (hs_s, hs_r)).start()

        @pl.when(b >= LAG)
        def _():
            hand_on(b - LAG)

    for d in range(1, tp_n):
        weight(d).wait()

    def finish(b):
        rows = rows_of(b, BLOCK)
        to_sib(ho_ref.at[tp], ho_ref, b, BLOCK, (hs_s, hs_r)).wait()
        for i in range(far):
            to_far(ho_ref.at[tp], ho_ref, b, BLOCK, i, (hx_s, hx_r)).wait_send()
            relay(ho_ref, b, BLOCK, i, (hr_s, hr_r)).wait()
        total = jnp.zeros((BLOCK, cols), jnp.float32)
        for t in range(tp_n):
            total = total + jnp.dot(ho_ref[t, rows, :], wc_ref[t], preferred_element_type=jnp.float32)
        proj_ref[rows, :] = total
        squares = jnp.sum(total * total, axis=1, keepdims=True)
        ss_ref[tp, pl.ds(b, 1), :] = jnp.broadcast_to(squares, (BLOCK, BLOCK)).T[0:1]

    for b in range(blocks - LAG, blocks):
        hand_on(b)
    pl.loop(0, blocks)(finish)

    def sums(d):
        return send(ss_ref.at[tp], ss_ref.at[tp], (s_s.at[d - 1], s_r.at[d - 1]), at_tp(lax.rem(tp + d, tp_n)))

    for d in range(1, tp_n):
        sums(d).start()
    for d in range(1, tp_n):
        sums(d).wait()
    total = ss_ref[0]
    for t in range(1, tp_n):
        total = total + ss_ref[t]
    rs_ref[...] = lax.rsqrt(total / (cols * tp_n) + epsilon)
    gains = ogain_ref[:, pl.ds(pl.multiple_of(tp * cols, cols), cols)]

    @pl.loop(0, blocks)
    def _(b):
        rows = rows_of(b, BLOCK)
        scale = jnp.broadcast_to(rs_ref[pl.ds(b, 1), :], (BLOCK, BLOCK)).T
        scale = jnp.concatenate([scale] * (cols // BLOCK), axis=1)
        o_ref[rows, :] = (proj_ref[rows, :] * scale * gains).astype(jnp.bfloat16)


def on_device(
    tokens,
    query_weight,
    latent_weight,
    query_gain,
    key_gain,
    value_up,
    out_weight,
    out_gain,
    chosen,
):
    toks, feat = tokens.shape
    width = latent_weight.shape[1]
    heads = query_weight.shape[1] // width
    blocks = toks // BLOCK
    kv_n, tp_n = lax.axis_size("kv"), lax.axis_size("tp")
    cols = out_weight.shape[1] // tp_n
    hv = out_weight.shape[0]
    far = tp_n // 2 - 1
    slots = blocks + (kv_n - 1) * PER_OWNER
    bf, f32 = jnp.bfloat16, jnp.float32
    wide = jnp.pad(chosen, ((0, 0), (0, BLOCK - chosen.shape[1])), constant_values=-1)
    scaled = (query_gain * (width**-0.5 * 1.4426950408889634))[None, :]
    dma = pltpu.SemaphoreType.DMA
    kvs, tps = [dma((kv_n - 1,))] * 2, [dma((tp_n - 1,))] * 2
    cs, cf = [dma((CHUNKS,))] * 2, [dma((far, CHUNKS))] * 2
    bs, bfar = [dma((blocks,))] * 2, [dma((far, blocks))] * 2
    return pl.pallas_call(
        functools.partial(kernel, kv_n, tp_n),
        out_shape=jax.ShapeDtypeStruct((toks, cols), bf),
        in_specs=[pl.BlockSpec(memory_space=pltpu.VMEM)] * 9,
        out_specs=pl.BlockSpec(memory_space=pltpu.VMEM),
        scratch_shapes=[
            pltpu.VMEM((tp_n, toks, feat), bf),
            pltpu.VMEM((toks, heads * width), bf),
            pltpu.VMEM((slots * BLOCK, width), bf),
            pltpu.VMEM((blocks, slots * BLOCK), f32),
            pltpu.VMEM((kv_n - 1, blocks, BLOCK), jnp.int32),
            pltpu.VMEM((kv_n - 1, BLOCK, width), bf),
            pltpu.VMEM((slots * BLOCK, width), bf),
            pltpu.VMEM((slots * BLOCK, 2 * width), bf),
            pltpu.VMEM((heads * BLOCK, slots * BLOCK), bf),
            pltpu.VMEM((tp_n, toks, hv), bf),
            pltpu.VMEM((tp_n, hv, cols), bf),
            pltpu.VMEM((toks, cols), f32),
            pltpu.VMEM((tp_n, blocks, BLOCK), f32),
            pltpu.VMEM((blocks, BLOCK), f32),
            *kvs, *cs, *cf, *cf, *kvs, *kvs, *bs, *bfar, *bfar, *tps, *tps,
        ],
        compiler_params=pltpu.CompilerParams(
            collective_id=0, has_side_effects=True, vmem_limit_bytes=60 << 20
        ),
    )(
        tokens, query_weight, latent_weight, scaled, key_gain[None, :], paired_up(value_up),
        out_weight, out_gain[None, :], wide,
    )


def solution(mesh):
    in_specs = (
        P("kv", "tp"),
        P(None, "tp"),
        P(),
        P(),
        P(),
        P("tp", None, None),
        P("tp", None),
        P(),
        P("kv", None),
    )
    out_specs = P("kv", "tp")
    return jax.shard_map(
        on_device, mesh=mesh, in_specs=in_specs, out_specs=out_specs, check_vma=False
    )
```

time: 133 us -> 62.3 us (0.47); the launches traced: 131 us -> 62.1 us
  waiting for transfers between devices: 46.8 us -> 0 us
  Pallas kernels: 20.3 us -> 56.6 us
  other arithmetic: 16.5 us -> 1.26 us
  between operations: 13.5 us -> 0.02 us
  starting transfers between devices: 10.9 us -> 0 us
  matrix products: 8.32 us -> 0 us
  blocking collectives: 5.95 us -> 0 us
  local copies, waits for them, and re-layouts: 8.45 us -> 4.16 us
    pallas_call x1, Pallas kernels: 20.3 us -> 56.6 us  [on_device(): pl.pallas_call(functools.partial(kernel, kv_n, tp_n), out_shape=jax.Shape...]
    reduce_scatter x1 -> x0, waiting for transfers between devices: 30.3 us -> none  [own_rows(): lax.psum_scatter(everything.astype(jnp.bfloat16), axis, scatter_dimension...]
    all_gather x1 -> x0, waiting for transfers between devices: 13.2 us -> none  [taken_in(): lax.all_gather(part, axis, axis=dim, tiled=True)]
    all_to_all x2 -> x0, starting transfers between devices: 10.9 us -> none  [the longest x1 5.44 us: on_device(): lax.all_to_all(wanted, 'kv', split_axis=0, concat_axis=0, tiled=True)]
    dot_general x3 -> x0, matrix products: 8.32 us -> none  [the longest x1 3.11 us: columns(): lax.dot_general(weight_cols, heads_out, (((0,), (1,)), ((), ())), preferr...]
    psum x1 -> x0, blocking collectives: 5.95 us -> none  [on_device(): squares = lax.psum(jnp.sum(summed * summed, axis=1), 'tp')]
    convert_element_type x3 -> x0, other arithmetic: 3.46 us -> none  [the longest x1 2.04 us: on_device(): (summed * lax.rsqrt(squares / model_width + epsilon)[:, None] * gain_part...]
    reduce_sum x3 -> x0, other arithmetic: 3.35 us -> none  [the longest x1 1.95 us: rms_scale(): mean_sq = jnp.mean(widened * widened, axis=-1, keepdims=True)]
  transfers between devices with their start and end apart: 4 -> 0, of which waited for: 3 -> 0; matrix products, arithmetic and copies ran while one was open for 14% -> 0% of each run, Pallas kernels for 0% -> 0%
where the time goes in v2:
time: 62.3 us; the launch traced here: 62.1 us
  Pallas kernels  56.6 us (91%)
  local copies, waits for them, and re-layouts  4.16 us (7%)
  other arithmetic  1.26 us (2%)
    pallas_call x1, Pallas kernels, on_device(): pl.pallas_call(functools.partial(kernel, kv_n, tp_n), out_shape=jax.Shape...  56.6 us
    unnamed x7, local copies, waits for them, and re-layouts  2.78 us

profile of v2, /device:TPU:29, one launch (start us, length us, event | category | flops | bytes accessed | tf_op | source)
XLA Modules:
  0.0 62.1 jit_solution(8427996163885610652)
XLA Ops:
  0.0 0.0 copy-start
  0.0 0.0 copy-start.1
  0.0 0.7 %copy-done.1 = f32[128]{0:T(128)S(1)} copy-done((f32[128]{0:T(128)S(1)}, f32[128]{0:T(128)}, u32[]{:S(2)}) %copy-start.1) | copy-done | bytes 536
  0.7 0.5 multiply_bitcast_fusion.qgain_ref
  1.2 0.0 copy-done
  1.2 0.6 pad.14.chosen_ref
  1.8 0.8 %fusion.3 = (bf16[2,1,128,64]{2,3,1,0:T(8,128)(2,1)S(1)}, bf16[2,1,128,64]{2,3,1,0:T(8,128)(2,1)S(1)}) fusion(bf16[2,2,128,64]{2,3,1,0:T(8,128)(2,1)} %bitcast.9), kind=kLoop, calls=%fused_computation.6 | loop fusion | bytes 131072 | tf_op jit(solution)/shard_map/slice | solution.py:65
  2.6 0.1 copy.12
  2.7 0.1 copy.13
  2.8 0.8 %fusion.2.vu_ref = bf16[2,256,128]{2,1,0:T(8,128)(2,1)} fusion(bf16[2,128,64]{2,1,0:T(8,128)(2,1)S(1)} %bitcast.8, bf16[2,128,64]{2,1,0:T(8,128)(2,1)S(1)} %bitcast.7), kind=kLoop, calls=%fused_computation.4 | loop fusion | flops 524288 | bytes 196608 | tf_op jit(solution)/shard_map/concatenate | solution.py:67
  3.6 56.6 %shard_map.91 = bf16[1024,256]{1,0:T(8,128)(2,1)} custom-call(bf16[1024,256]{1,0:T(8,128)(2,1)} %tok_ref.1, bf16[1024,512]{1,0:T(8,128)(2,1)} %wq_ref.1, bf16[1024,128]{1,0:T(8,128)(2,1)} %wl_ref.1, f32[1,128]{1,0:T(1,128)} %multiply_bitcast_fusion.qgain_ref, f32[1,128]{1,0:T(1,128)} %bitcast.11, bf16[2,256,128]{2,1,0:T(8,128)(2,1)} %fusion.2.vu_ref, ...), custom_call_target="tpu_custom_call" | custom-call | tf_op jit(solution)/shard_map/pallas_call | solution.py:351
  60.2 1.9 %copy.15 = bf16[1024,256]{1,0:T(8,128)(2,1)} copy(bf16[1024,256]{1,0:T(8,128)(2,1)} %shard_map.91) | data formatting | bytes 1048576
Async XLA Ops:
  0.0 1.2 %copy-start = (s32[8,32]{1,0:T(8,128)S(1)}, s32[8,32]{1,0:T(8,128)}, u32[]{:S(2)}) copy-start(s32[8,32]{1,0:T(8,128)} %param.17) | copy-start | bytes 3076
  0.0 0.7 %copy-start.1 = (f32[128]{0:T(128)S(1)}, f32[128]{0:T(128)}, u32[]{:S(2)}) copy-start(f32[128]{0:T(128)} %param.12) | copy-start | bytes 1540
